TPU v7x, 32 devices: a whole 2x2x4 slice. The times are simulated.
32 devices in a mesh: sp: 8 (over z, y), dp: 4 (over x, core).
Axes of the slice: x: 2, y: 2, z: 4, core: 2. Of those that a mesh axis runs over, the one named last changes fastest.
Arguments:
- tokens: bfloat16 [4, 2048, 2048], P('dp', 'sp'), may hold values from -6 to 6
- w_query: bfloat16 [2048, 2048], P('dp', 'sp'), may hold values from -0.125 to 0.125
- w_key: bfloat16 [2048, 1024], P('dp', 'sp'), may hold values from -0.125 to 0.125
- w_value: bfloat16 [2048, 1024], P('dp', 'sp'), may hold values from -0.125 to 0.125
- w_out: bfloat16 [2048, 2048], P('dp', 'sp'), may hold values from -0.25 to 0.25
- qk_gain: float32 [2, 128], replicated, may hold values from 0.9 to 24
Outputs:
- mixed_out: bfloat16 [4, 2048, 2048], P('dp', 'sp')
All inputs are finite; a program needn't handle non-finite values.
Results may differ from a plain program's by a relative error of at most 0.006.
The roundings to bfloat16 on the way count: a program that leaves them out, or rounds other values in their place, can miss the bound.
Values may be sent and summed in bfloat16 or wider, within the bound.
A program may use at most 64 MiB of HBM per device.

v0:
```python
import math
import jax
import jax.numpy as jnp
import numpy as np
from jax import lax
from jax.sharding import PartitionSpec as P

HQ = 16
KV = 8
HD = 128
GRID_W = 64
ROPE_BASE = 10000.0
EPS = 1e-06


def angles(positions):
    quarter = jnp.arange(0, HD // 2, 2, dtype=jnp.float32)
    inv_freq = ROPE_BASE ** (-quarter / (HD // 2))
    row_pos = (positions // GRID_W).astype(jnp.float32)
    col_pos = (positions % GRID_W).astype(jnp.float32)
    angle_table = jnp.concatenate(
        [row_pos[:, None] * inv_freq, col_pos[:, None] * inv_freq], axis=1
    )
    return (jnp.cos(angle_table), jnp.sin(angle_table))


def prepare(raw_proj, gain_row, cosine, sine_table):
    normed = (
        raw_proj * lax.rsqrt(jnp.mean(raw_proj * raw_proj, axis=-1, keepdims=True) + EPS) * gain_row
    )
    pair_view = normed.reshape(raw_proj.shape[:-1] + (HD // 2, 2))
    first_half = pair_view[..., 0]
    second = pair_view[..., 1]
    cos_b = cosine[:, None, :]
    sin_b = sine_table[:, None, :]
    turned = jnp.stack(
        [first_half * cos_b - second * sin_b, first_half * sin_b + second * cos_b], axis=-1
    )
    return turned.reshape(raw_proj.shape).astype(jnp.bfloat16)


def attend_head(query_rows, key_rows, value_rows):
    seq_len = query_rows.shape[0]
    block_len = math.gcd(seq_len, 512)
    blocks = query_rows.reshape(seq_len // block_len, block_len, HD)

    def one_block(row_block):
        scores = jnp.dot(row_block, key_rows.T, preferred_element_type=jnp.float32) * HD ** (-0.5)
        top_score = jnp.max(scores, axis=1, keepdims=True)
        weights = jnp.exp(scores - top_score)
        row_total = jnp.sum(weights, axis=1, keepdims=True)
        probs_bf = (weights / row_total).astype(jnp.bfloat16)
        return jnp.dot(probs_bf, value_rows, preferred_element_type=jnp.float32).astype(
            jnp.bfloat16
        )

    return lax.map(one_block, blocks).reshape(seq_len, HD)


def project(own_rows, weight):
    col_full = lax.all_gather(weight, "sp", axis=1, tiled=True)
    return jnp.dot(
        own_rows,
        lax.all_gather(col_full, "dp", axis=0, tiled=True),
        preferred_element_type=jnp.float32,
    )


def on_device(tokens, w_query, w_key, w_value, w_out, qk_gain):
    own_rows = tokens[0]
    n_seqdev = lax.axis_size("sp")
    tok_local = own_rows.shape[0]
    positions = lax.axis_index("sp") * tok_local + jnp.arange(tok_local, dtype=jnp.int32)
    cosine, sine_table = angles(positions)
    heads_dev = HQ // n_seqdev
    group_size = HQ // KV
    kv_dev = max(1, heads_dev // group_size)
    chosen = (np.arange(n_seqdev) * heads_dev // group_size)[:, None] + np.arange(kv_dev)[None, :]
    chosen = chosen.reshape(-1)
    key_all = prepare(
        project(own_rows, w_key).reshape(tok_local, KV, HD), qk_gain[1], cosine, sine_table
    )
    values = project(own_rows, w_value).astype(jnp.bfloat16).reshape(tok_local, KV, HD)
    key_send = key_all[:, chosen, :].reshape(tok_local, -1)
    value_send = values[:, chosen, :].reshape(tok_local, -1)
    raw_proj = project(own_rows, w_query).reshape(tok_local, HQ, HD)
    query_heads = lax.all_to_all(
        prepare(raw_proj, qk_gain[0], cosine, sine_table).reshape(tok_local, HQ * HD),
        "sp",
        split_axis=1,
        concat_axis=0,
        tiled=True,
    )
    key_heads = lax.all_to_all(key_send, "sp", split_axis=1, concat_axis=0, tiled=True)
    value_heads = lax.all_to_all(value_send, "sp", split_axis=1, concat_axis=0, tiled=True)
    outputs = []
    for head_index in range(heads_dev):
        kv_slot = head_index // group_size if heads_dev >= group_size else 0
        outputs.append(
            attend_head(
                query_heads[:, head_index * HD : (head_index + 1) * HD],
                key_heads[:, kv_slot * HD : (kv_slot + 1) * HD],
                value_heads[:, kv_slot * HD : (kv_slot + 1) * HD],
            )
        )
    mixed_heads = jnp.concatenate(outputs, axis=1)
    token_rows = lax.all_to_all(mixed_heads, "sp", split_axis=0, concat_axis=1, tiled=True)
    return project(token_rows, w_out).astype(jnp.bfloat16)[None]


def solution(mesh):
    in_specs = (
        P("dp", "sp", None),
        P("dp", "sp"),
        P("dp", "sp"),
        P("dp", "sp"),
        P("dp", "sp"),
        P(),
    )
    out_specs = P("dp", "sp", None)
    return jax.shard_map(
        on_device, mesh=mesh, in_specs=in_specs, out_specs=out_specs, check_vma=False
    )
```

profile of v0, /device:TPU:0, one launch (start us, length us, event | category | flops | bytes accessed | tf_op | source)
XLA Modules:
  0.0 416.6 jit_solution(12027826076929534750)
XLA Ops:
  6.5 0.7 all-gather.17.cloned.1.call-update
  7.3 0.7 all-gather.9.cloned.1.call-update
  8.1 0.7 all-gather.13.cloned.1.call-update
  8.8 42.7 %all-gather.17.cloned.1.call-done = bf16[512,1024]{1,0:T(8,128)(2,1)} async-done(((bf16[512,128]{1,0:T(8,128)(2,1)}), bf16[512,1024]{1,0:T(8,128)(2,1)}) %all-gather.17.cloned.1.call-update) | async-done | bytes 1048592 | tf_op jit(solution)/shard_map/all_gather | solution.py:61
  51.6 51.4 %all-gather.9.cloned.1.call-done = bf16[512,2048]{1,0:T(8,128)(2,1)} async-done(((bf16[512,256]{1,0:T(8,128)(2,1)}), bf16[512,2048]{1,0:T(8,128)(2,1)}) %all-gather.9.cloned.1.call-update) | async-done | bytes 2097168 | tf_op jit(solution)/shard_map/all_gather | solution.py:61
  103.0 39.6 %all-gather.13.cloned.1.call-done = bf16[512,1024]{1,0:T(8,128)(2,1)} async-done(((bf16[512,128]{1,0:T(8,128)(2,1)}), bf16[512,1024]{1,0:T(8,128)(2,1)}) %all-gather.13.cloned.1.call-update) | async-done | bytes 1048592 | tf_op jit(solution)/shard_map/all_gather | solution.py:61
  142.7 0.7 all-gather.21.cloned.1.call-update
  143.6 0.2 fusion.28
  143.8 33.7 %all-gather.19.cloned.1.call-done = bf16[2048,1024]{1,0:T(8,128)(2,1)} async-done(((bf16[512,1024]{1,0:T(8,128)(2,1)}), bf16[2048,1024]{1,0:T(8,128)(2,1)}) %all-gather.19.cloned.1.call-update) | async-done | bytes 4194320 | tf_op jit(solution)/shard_map/all_gather | solution.py:64
  177.6 3.4 fusion.21
  181.0 0.1 copy.30
  181.1 1.5 gather_fusion.1
  182.6 5.5 %all-to-all-start.2 = ((bf16[256,8,128]{2,0,1:T(8,128)(2,1)}), bf16[256,8,128]{2,0,1:T(8,128)(2,1)}, u32[]{:S(2)}, u32[]{:S(2)}) async-start(bf16[256,8,128]{2,0,1:T(8,128)(2,1)} %bitcast.19), calls=%async_computation.2 | async-start | bytes 1048576 | tf_op jit(solution)/shard_map/all_to_all | solution.py:95
  188.1 49.2 %all-gather.11.cloned.1.call-done = bf16[2048,2048]{1,0:T(8,128)(2,1)} async-done(((bf16[512,2048]{1,0:T(8,128)(2,1)}), bf16[2048,2048]{1,0:T(8,128)(2,1)}) %all-gather.11.cloned.1.call-update) | async-done | bytes 8388624 | tf_op jit(solution)/shard_map/all_gather | solution.py:64
  237.3 12.2 %copy.19 = bf16[2048,2048]{1,0:T(8,128)(2,1)} copy(bf16[2048,2048]{0,1:T(8,128)(2,1)} %bitcast.93) | data formatting | bytes 16777216 | tf_op jit(solution)/shard_map/dot_general | solution.py:62
  249.5 5.8 %multiply_reduce_fusion.2 = (f32[256,16]{0,1:T(8,128)S(1)}, f32[256,16,128]{0,2,1:T(8,128)S(1)}) fusion(bf16[16,128,2048]{2,1,0:T(8,128)(2,1)} %bitcast.94, bf16[1,256,2048]{2,1,0:T(8,128)(2,1)S(1)} %copy-done), kind=kOutput, calls=%fused_computation.31 | convolution fusion | flops 2148528128 | bytes 11550720 | tf_op jit(solution)/shard_map/dot_general | solution.py:62
  255.3 1.7 multiply_multiply_fusion
  257.0 2.5 reshape.165
  259.5 2.9 subtract_convert_fusion
  262.4 2.4 pad_maximum_fusion
  264.8 1.2 convert_element_type.44
  266.1 5.5 %all-to-all-start = ((bf16[256,8,256]{0,2,1:T(8,128)(2,1)}), bf16[256,8,256]{0,2,1:T(8,128)(2,1)S(1)}, u32[]{:S(2)}, u32[]{:S(2)}) async-start(bf16[256,8,256]{0,2,1:T(8,128)(2,1)} %convert_element_type.44), calls=%async_computation | async-start | bytes 2097152 | tf_op jit(solution)/shard_map/all_to_all | solution.py:87
  271.6 1.6 all-gather.15.cloned.1.call-done
  273.2 6.5 %copy.21 = bf16[1024,2048]{1,0:T(8,128)(2,1)} copy(bf16[1024,2048]{0,1:T(8,128)(2,1)} %bitcast.96) | data formatting | bytes 8388608 | tf_op jit(solution)/shard_map/dot_general | solution.py:62
  279.7 3.5 multiply_reduce_fusion.3
  283.2 0.2 multiply_multiply_fusion.1
  283.4 0.6 copy.27
  284.0 0.1 subtract_convert_fusion.1
  284.2 0.4 copy.24
  284.7 1.4 gather_fusion
  286.1 20.1 %all-to-all-done = bf16[256,8,256]{0,2,1:T(8,128)(2,1)S(1)} async-done(((bf16[256,8,256]{0,2,1:T(8,128)(2,1)}), bf16[256,8,256]{0,2,1:T(8,128)(2,1)S(1)}, u32[]{:S(2)}, u32[]{:S(2)}) %all-to-all-start) | async-done | bytes 1048608 | tf_op jit(solution)/shard_map/all_to_all | solution.py:87
  306.2 3.5 all-to-all-start.1
  309.8 31.3 %all-gather.21.cloned.1.call-done = bf16[512,2048]{1,0:T(8,128)(2,1)} async-done(((bf16[512,256]{1,0:T(8,128)(2,1)}), bf16[512,2048]{1,0:T(8,128)(2,1)}) %all-gather.21.cloned.1.call-update) | async-done | bytes 2097168 | tf_op jit(solution)/shard_map/all_gather | solution.py:61
  341.1 0.5 copy.20
  341.8 15.1 %while.21 = (s32[]{:T(128)}, bf16[4,512,128]{2,1,0:T(8,128)(2,1)S(1)}, bf16[4,512,128]{2,1,0:T(8,128)(2,1)S(1)}, bf16[2048,128]{1,0:T(8,128)(2,1)S(1)}, bf16[2048,128]{1,0:T(8,128)(2,1)}, /*index=5*/s32[]{:T(128)}) while((s32[]{:T(128)}, bf16[4,512,128]{2,1,0:T(8,128)(2,1)S(1)}, bf16[4,512,128]{2,1,0:T(8,128)(2,1)S(1)}, ...), condition=%wide.region_9.10_spmd, body=%wide.region_6.9_spmd.sunk | while | flops 546372608 | bytes 13903957 | solution.py:57
  341.8 0.8 multiply_reduce_fusion.7
  342.6 0.8 fusion.56
  343.4 2.1 fusion.57
  345.5 0.8 multiply_reduce_fusion.7
  346.3 0.8 fusion.56
  347.2 2.2 fusion.57
  349.3 0.8 multiply_reduce_fusion.7
  350.1 0.8 fusion.56
  350.9 2.2 fusion.57
  353.2 0.8 multiply_reduce_fusion.7
  354.0 0.8 fusion.56
  354.8 2.1 fusion.57
  357.0 14.9 %while.20 = (s32[]{:T(128)}, bf16[4,512,128]{2,1,0:T(8,128)(2,1)S(1)}, bf16[4,512,128]{2,1,0:T(8,128)(2,1)S(1)}, bf16[2048,128]{1,0:T(8,128)(2,1)S(1)}, bf16[2048,128]{1,0:T(8,128)(2,1)}, /*index=5*/s32[]{:T(128)}) while((s32[]{:T(128)}, bf16[4,512,128]{2,1,0:T(8,128)(2,1)S(1)}, bf16[4,512,128]{2,1,0:T(8,128)(2,1)S(1)}, ...), condition=%wide.region_5.6_spmd, body=%wide.region_2.5_spmd.sunk | while | flops 546372608 | bytes 13903957 | solution.py:57
  357.0 0.8 multiply_reduce_fusion.6
  357.8 0.8 fusion.52
  358.6 2.1 fusion.53
  360.7 0.8 multiply_reduce_fusion.6
  361.5 0.8 fusion.52
  362.3 2.1 fusion.53
  364.5 0.8 multiply_reduce_fusion.6
  365.2 0.8 fusion.52
  366.1 2.1 fusion.53
  368.2 0.8 multiply_reduce_fusion.6
  369.0 0.8 fusion.52
  369.8 2.1 fusion.53
  371.9 0.1 pad_maximum_fusion.1
  372.0 30.4 %all_to_all.64 = bf16[8,256,256]{2,1,0:T(8,128)(2,1)S(1)} all-to-all(bf16[8,256,256]{2,1,0:T(8,128)(2,1)S(1)} %pad_maximum_fusion.1), channel_id=1, replica_groups=mesh['sp'=8,'dp'=4] {'sp'}, dimensions={0} | all-to-all | bytes 2097152 | tf_op jit(solution)/shard_map/all_to_all | solution.py:107
  402.4 0.5 copy.26
  403.0 6.8 %fusion.20 = bf16[1,256,2048]{2,1,0:T(8,128)(2,1)} fusion(bf16[256,2048]{0,1:T(8,128)(2,1)S(1)} %bitcast.95, bf16[2048,2048]{1,0:T(8,128)(2,1)} %all-gather.23.cloned.1.call-done), kind=kOutput, calls=%fused_computation.29 | convolution fusion | flops 2148007936 | bytes 10485760 | tf_op jit(solution)/shard_map/dot_general | solution.py:62
  (33 shorter events, 0.8 us)
Async XLA Ops:
  6.5 171.0 %copy-start = (bf16[1,256,2048]{2,1,0:T(8,128)(2,1)S(1)}, bf16[1,256,2048]{2,1,0:T(8,128)(2,1)}, u32[]{:S(2)}) copy-start(bf16[1,256,2048]{2,1,0:T(8,128)(2,1)} %param.13) | copy-start | bytes 3145732
  6.5 136.9 %copy-start.2 = (f32[2,128]{1,0:T(2,128)S(1)}, f32[2,128]{1,0:T(2,128)}, u32[]{:S(2)}) copy-start(f32[2,128]{1,0:T(2,128)} %param.18) | copy-start | bytes 3076
  6.5 45.0 %all-gather.17.cloned.1.call-start = ((), (), s32[]{:S(2)}) async-start(), calls=%async_computation.8 | async-start | bytes 1179648 | tf_op jit(solution)/shard_map/all_gather | solution.py:61
  7.3 95.7 %all-gather.9.cloned.1.call-start = ((), (), s32[]{:S(2)}) async-start(), calls=%async_computation.4 | async-start | bytes 2359296 | tf_op jit(solution)/shard_map/all_gather | solution.py:61
  8.0 134.6 %all-gather.13.cloned.1.call-start = ((), (), s32[]{:S(2)}) async-start(), calls=%async_computation.6 | async-start | bytes 1179648 | tf_op jit(solution)/shard_map/all_gather | solution.py:61
  8.7 168.8 %all-gather.19.cloned.1.call-start = ((), (), s32[]{:S(2)}) async-start(), calls=%async_computation.9 | async-start | bytes 5242880 | tf_op jit(solution)/shard_map/all_gather | solution.py:64
  51.6 185.7 %all-gather.11.cloned.1.call-start = ((), (), s32[]{:S(2)}) async-start(), calls=%async_computation.5 | async-start | bytes 10485760 | tf_op jit(solution)/shard_map/all_gather | solution.py:64
  103.0 170.2 %all-gather.15.cloned.1.call-start = ((), (), s32[]{:S(2)}) async-start(), calls=%async_computation.7 | async-start | bytes 5242880 | tf_op jit(solution)/shard_map/all_gather | solution.py:64
  142.7 198.4 %all-gather.21.cloned.1.call-start = ((), (), s32[]{:S(2)}) async-start(), calls=%async_computation.10 | async-start | bytes 2359296 | tf_op jit(solution)/shard_map/all_gather | solution.py:61
  182.6 83.5 %all-to-all-start.2 = ((bf16[256,8,128]{2,0,1:T(8,128)(2,1)}), bf16[256,8,128]{2,0,1:T(8,128)(2,1)}, u32[]{:S(2)}, u32[]{:S(2)}) async-start(bf16[256,8,128]{2,0,1:T(8,128)(2,1)} %bitcast.19), calls=%async_computation.2 | async-start | bytes 1048576 | tf_op jit(solution)/shard_map/all_to_all | solution.py:95
  266.1 40.1 %all-to-all-start = ((bf16[256,8,256]{0,2,1:T(8,128)(2,1)}), bf16[256,8,256]{0,2,1:T(8,128)(2,1)S(1)}, u32[]{:S(2)}, u32[]{:S(2)}) async-start(bf16[256,8,256]{0,2,1:T(8,128)(2,1)} %convert_element_type.44), calls=%async_computation | async-start | bytes 2097152 | tf_op jit(solution)/shard_map/all_to_all | solution.py:87
  306.2 35.5 %all-to-all-start.1 = ((bf16[256,8,128]{2,0,1:T(8,128)(2,1)}), bf16[256,8,128]{2,0,1:T(8,128)(2,1)S(1)}, u32[]{:S(2)}, u32[]{:S(2)}) async-start(bf16[256,8,128]{2,0,1:T(8,128)(2,1)} %bitcast.16), calls=%async_computation.1 | async-start | bytes 1048576 | tf_op jit(solution)/shard_map/all_to_all | solution.py:94
  309.7 93.2 %all-gather.23.cloned.1.call-start = ((), (), s32[]{:S(2)}) async-start(), calls=%async_computation.11 | async-start | bytes 10485760 | tf_op jit(solution)/shard_map/all_gather | solution.py:64
  403.0 6.8 %copy-start.1 = (bf16[1,256,2048]{2,1,0:T(8,128)(2,1)S(1)}, bf16[1,256,2048]{2,1,0:T(8,128)(2,1)}, u32[]{:S(2)}) copy-start(bf16[1,256,2048]{2,1,0:T(8,128)(2,1)} %param.13) | copy-start | bytes 3145732
Sparse Core Ops, SparseCore 0:
  9.4 42.1 all-gather.16
  53.6 49.3 all-gather.8
  105.0 37.5 all-gather.12
  144.0 33.4 all-gather.18
  179.0 58.2 all-gather.10
  238.7 34.4 all-gather.14
  275.2 65.8 all-gather.20
  342.6 57.7 all-gather.22
where the time goes:
time: 418 us; the launch traced here: 417 us
  waiting for transfers between devices  273 us (65%)
  matrix products  42.8 us (10%)
  blocking collectives  30.4 us (7%)
  local copies, waits for them, and re-layouts  27.8 us (7%)
  starting transfers between devices  14.8 us (4%)
  other arithmetic  14.5 us (3%)
  between operations  13.7 us (3%)
    all_gather x4, waiting for transfers between devices, project(): col_full = lax.all_gather(weight, 'sp', axis=1, tiled=True)  165 us
    all_gather x4, waiting for transfers between devices, project(): lax.all_gather(col_full, 'dp', axis=0, tiled=True)  84.5 us
    all_to_all x1, blocking collectives, on_device(): lax.all_to_all(mixed_heads, 'sp', split_axis=0, concat_axis=1, tiled=True)  30.4 us
    all_to_all x1, waiting for transfers between devices, on_device(): lax.all_to_all(prepare(raw_proj, qk_gain[0], cosine, sine_table).reshape(...  20.1 us
    dot_general x4, matrix products, project(): jnp.dot(own_rows, lax.all_gather(col_full, 'dp', axis=0, tiled=True), pre...  19.5 us
    dot_general x2, local copies, waits for them, and re-layouts, project(): jnp.dot(own_rows, lax.all_gather(col_full, 'dp', axis=0, tiled=True), pre...  18.7 us
    dot_general x8, matrix products, one_block(): jnp.dot(probs_bf, value_rows, preferred_element_type=jnp.float32)  17 us
  transfers between devices with their start and end apart: 11, of which 8 were waited for; matrix products, arithmetic and copies ran while one was open for 19% of the time, Pallas kernels for 0%

commit v1 on v0

--- a/solution.py
+++ b/solution.py
@@ -58,7 +58,7 @@
 
 
 def project(own_rows, weight):
-    col_full = lax.all_gather(weight, "sp", axis=1, tiled=True)
+    col_full = jnp.concatenate(lax.all_gather(weight, "sp"), axis=1)
     return jnp.dot(
         own_rows,
         lax.all_gather(col_full, "dp", axis=0, tiled=True),

time: 418 us -> 405 us (0.969)
  matrix products: 42.8 us -> 34.3 us
  local copies, waits for them, and re-layouts: 27.8 us -> 23.3 us
    dot_general x2 -> x0, local copies, waits for them, and re-layouts: 18.7 us -> none  [project(): jnp.dot(own_rows, lax.all_gather(col_full, 'dp', axis=0, tiled=True), pre...]
    reshape x0 -> x4, local copies, waits for them, and re-layouts: none -> 12.4 us  [project(): col_full = jnp.concatenate(lax.all_gather(weight, 'sp'), axis=1)]
    all_gather x4, waiting for transfers between devices: 84.5 us -> 94.6 us  [project(): lax.all_gather(col_full, 'dp', axis=0, tiled=True)]
    dot_general x8, matrix products: 17 us -> 8.4 us  [one_block(): jnp.dot(probs_bf, value_rows, preferred_element_type=jnp.float32)]
    all_to_all x1, waiting for transfers between devices: 20.1 us -> 13.2 us  [on_device(): lax.all_to_all(prepare(raw_proj, qk_gain[0], cosine, sine_table).reshape(...]
  transfers between devices with their start and end apart: 11 -> 11, of which waited for: 8 -> 9; matrix products, arithmetic and copies ran while one was open for 19% -> 16% of each run, Pallas kernels for 0% -> 0%
where the time goes in v1:
time: 405 us; the launch traced here: 404 us
  waiting for transfers between devices  273 us (67%)
  matrix products  34.3 us (8%)
  blocking collectives  28.8 us (7%)
  local copies, waits for them, and re-layouts  23.3 us (6%)
  other arithmetic  15.9 us (4%)
  starting transfers between devices  14.9 us (4%)
  between operations  13.7 us (3%)
    all_gather x4, waiting for transfers between devices, project(): col_full = jnp.concatenate(lax.all_gather(weight, 'sp'), axis=1)  163 us
    all_gather x4, waiting for transfers between devices, project(): lax.all_gather(col_full, 'dp', axis=0, tiled=True)  94.6 us
    all_to_all x1, blocking collectives, on_device(): lax.all_to_all(mixed_heads, 'sp', split_axis=0, concat_axis=1, tiled=True)  28.8 us
    dot_general x4, matrix products, project(): jnp.dot(own_rows, lax.all_gather(col_full, 'dp', axis=0, tiled=True), pre...  19.6 us
    all_to_all x1, waiting for transfers between devices, on_device(): lax.all_to_all(prepare(raw_proj, qk_gain[0], cosine, sine_table).reshape(...  13.2 us
    reshape x4, local copies, waits for them, and re-layouts, project(): col_full = jnp.concatenate(lax.all_gather(weight, 'sp'), axis=1)  12.4 us
    dot_general x8, matrix products, one_block(): jnp.dot(probs_bf, value_rows, preferred_element_type=jnp.float32)  8.4 us
  transfers between devices with their start and end apart: 11, of which 9 were waited for; matrix products, arithmetic and copies ran while one was open for 16% of the time, Pallas kernels for 0%

profile of v1, /device:TPU:0, one launch (start us, length us, event | category | flops | bytes accessed | tf_op | source)
XLA Modules:
  0.0 404.2 jit_solution(3382594581786282505)
XLA Ops:
  6.5 0.7 all-gather.23.cloned.1.call-update
  7.3 0.7 all-gather.21.cloned.1.call-update
  8.1 0.7 all-gather.25.cloned.1.call-update
  8.8 43.7 %all-gather.23.cloned.1.call-done = bf16[4096,128]{1,0:T(8,128)(2,1)} async-done(((bf16[512,128]{1,0:T(8,128)(2,1)}), bf16[4096,128]{1,0:T(8,128)(2,1)}) %all-gather.23.cloned.1.call-update) | async-done | bytes 1048592 | tf_op jit(solution)/shard_map/all_gather | solution.py:61
  52.5 2.3 copy.21
  54.8 47.6 %all-gather.21.cloned.1.call-done = bf16[4096,256]{1,0:T(8,128)(2,1)} async-done(((bf16[512,256]{1,0:T(8,128)(2,1)}), bf16[4096,256]{1,0:T(8,128)(2,1)}) %all-gather.21.cloned.1.call-update) | async-done | bytes 2097168 | tf_op jit(solution)/shard_map/all_gather | solution.py:61
  102.4 3.9 copy.19
  106.5 37.0 %all-gather.25.cloned.1.call-done = bf16[4096,128]{1,0:T(8,128)(2,1)} async-done(((bf16[512,128]{1,0:T(8,128)(2,1)}), bf16[4096,128]{1,0:T(8,128)(2,1)}) %all-gather.25.cloned.1.call-update) | async-done | bytes 1048592 | tf_op jit(solution)/shard_map/all_gather | solution.py:61
  143.4 2.3 copy.25
  145.8 0.7 all-gather.27.cloned.1.call-update
  146.6 0.2 fusion.28
  146.9 31.2 %all-gather.15.cloned.1.call-done = bf16[2048,1024]{0,1:T(8,128)(2,1)} async-done(((bf16[512,1024]{0,1:T(8,128)(2,1)}), bf16[2048,1024]{0,1:T(8,128)(2,1)}) %all-gather.15.cloned.1.call-update) | async-done | bytes 4194320 | tf_op jit(solution)/shard_map/all_gather | solution.py:64
  178.0 3.5 multiply_reduce_fusion.3
  181.8 0.6 copy.29
  182.6 0.4 copy.24
  183.0 1.4 gather_fusion
  184.5 5.5 %all-to-all-start.1 = ((bf16[256,8,128]{2,0,1:T(8,128)(2,1)}), bf16[256,8,128]{2,0,1:T(8,128)(2,1)S(1)}, u32[]{:S(2)}, u32[]{:S(2)}) async-start(bf16[256,8,128]{2,0,1:T(8,128)(2,1)} %bitcast.22), calls=%async_computation.1 | async-start | bytes 1048576 | tf_op jit(solution)/shard_map/all_to_all | solution.py:94
  190.0 47.8 %all-gather.13.cloned.1.call-done = bf16[2048,2048]{0,1:T(8,128)(2,1)} async-done(((bf16[512,2048]{0,1:T(8,128)(2,1)}), bf16[2048,2048]{0,1:T(8,128)(2,1)}) %all-gather.13.cloned.1.call-update) | async-done | bytes 8388624 | tf_op jit(solution)/shard_map/all_gather | solution.py:64
  237.7 5.8 %multiply_reduce_fusion.2 = (f32[256,16]{0,1:T(8,128)S(1)}, f32[256,16,128]{0,2,1:T(8,128)S(1)}) fusion(bf16[16,128,2048]{2,1,0:T(8,128)(2,1)} %bitcast.131, bf16[1,256,2048]{2,1,0:T(8,128)(2,1)S(1)} %copy-done), kind=kOutput, calls=%fused_computation.31 | convolution fusion | flops 2148528128 | bytes 11550720 | tf_op jit(solution)/shard_map/dot_general | solution.py:62
  243.6 1.7 multiply_multiply_fusion
  245.2 3.6 reshape.191
  248.8 4.3 %subtract_convert_fusion = (bf16[256,16,64,1]{0,3,2,1:T(2,128)(2,1)S(1)}, bf16[256,16,64,1]{0,3,2,1:T(2,128)(2,1)S(1)}) fusion(f32[256,16,64,2]{0,3,2,1:T(2,128)} %reshape.191, f32[256,64]{0,1:T(8,128)S(1)} %get-tuple-element.92, f32[256,64]{0,1:T(8,128)S(1)} %get-tuple-element.91), kind=kLoop, calls=%fused_computation.44 | loop fusion | flops 2097152 | bytes 3276800 | tf_op jit(solution)/shard_map/convert.2
  253.1 2.4 pad_maximum_fusion
  255.6 1.2 convert_element_type.44
  256.8 5.6 %all-to-all-start = ((bf16[256,8,256]{0,2,1:T(8,128)(2,1)}), bf16[256,8,256]{0,2,1:T(8,128)(2,1)S(1)}, u32[]{:S(2)}, u32[]{:S(2)}) async-start(bf16[256,8,256]{0,2,1:T(8,128)(2,1)} %convert_element_type.44), calls=%async_computation | async-start | bytes 2097152 | tf_op jit(solution)/shard_map/all_to_all | solution.py:87
  262.4 11.3 %all-gather.17.cloned.1.call-done = bf16[2048,1024]{0,1:T(8,128)(2,1)} async-done(((bf16[512,1024]{0,1:T(8,128)(2,1)}), bf16[2048,1024]{0,1:T(8,128)(2,1)}) %all-gather.17.cloned.1.call-update) | async-done | bytes 4194320 | tf_op jit(solution)/shard_map/all_gather | solution.py:64
  273.7 3.5 fusion.21
  277.2 1.4 gather_fusion.1
  278.6 13.2 %all-to-all-done = bf16[256,8,256]{0,2,1:T(8,128)(2,1)S(1)} async-done(((bf16[256,8,256]{0,2,1:T(8,128)(2,1)}), bf16[256,8,256]{0,2,1:T(8,128)(2,1)S(1)}, u32[]{:S(2)}, u32[]{:S(2)}) %all-to-all-start) | async-done | bytes 1048608 | tf_op jit(solution)/shard_map/all_to_all | solution.py:87
  291.8 3.5 all-to-all-start.2
  295.4 34.2 %all-gather.27.cloned.1.call-done = bf16[4096,256]{1,0:T(8,128)(2,1)} async-done(((bf16[512,256]{1,0:T(8,128)(2,1)}), bf16[4096,256]{1,0:T(8,128)(2,1)}) %all-gather.27.cloned.1.call-update) | async-done | bytes 2097168 | tf_op jit(solution)/shard_map/all_gather | solution.py:61
  329.6 4.0 copy.28
  333.6 0.5 copy.20
  334.2 0.8 copy-done.2
  335.1 10.8 %while.20 = (s32[]{:T(128)}, bf16[4,512,128]{2,1,0:T(8,128)(2,1)S(1)}, bf16[4,512,128]{2,1,0:T(8,128)(2,1)S(1)}, bf16[2048,128]{1,0:T(8,128)(2,1)S(1)}, bf16[2048,128]{1,0:T(8,128)(2,1)}, /*index=5*/s32[]{:T(128)}) while((s32[]{:T(128)}, bf16[4,512,128]{2,1,0:T(8,128)(2,1)S(1)}, bf16[4,512,128]{2,1,0:T(8,128)(2,1)S(1)}, ...), condition=%wide.region_5.6_spmd, body=%wide.region_2.5_spmd.sunk | while | flops 546372608 | bytes 16001129 | solution.py:57
  335.1 0.8 multiply_reduce_fusion.6
  335.9 0.8 fusion.52
  336.7 1.1 fusion.53
  337.8 0.8 multiply_reduce_fusion.6
  338.6 0.8 fusion.52
  339.4 1.0 fusion.53
  340.5 0.8 multiply_reduce_fusion.6
  341.3 0.8 fusion.52
  342.1 1.0 fusion.53
  343.2 0.8 multiply_reduce_fusion.6
  344.0 0.8 fusion.52
  344.8 1.0 fusion.53
  345.9 10.8 %while.21 = (s32[]{:T(128)}, bf16[4,512,128]{2,1,0:T(8,128)(2,1)S(1)}, bf16[4,512,128]{2,1,0:T(8,128)(2,1)S(1)}, bf16[2048,128]{1,0:T(8,128)(2,1)S(1)}, bf16[2048,128]{1,0:T(8,128)(2,1)}, /*index=5*/s32[]{:T(128)}) while((s32[]{:T(128)}, bf16[4,512,128]{2,1,0:T(8,128)(2,1)S(1)}, bf16[4,512,128]{2,1,0:T(8,128)(2,1)S(1)}, ...), condition=%wide.region_9.10_spmd, body=%wide.region_6.9_spmd.sunk | while | flops 546372608 | bytes 16001129 | solution.py:57
  346.0 0.8 multiply_reduce_fusion.7
  346.7 0.8 fusion.56
  347.6 1.1 fusion.57
  348.7 0.8 multiply_reduce_fusion.7
  349.4 0.8 fusion.56
  350.3 1.1 fusion.57
  351.3 0.8 multiply_reduce_fusion.7
  352.1 0.8 fusion.56
  353.0 1.1 fusion.57
  354.0 0.8 multiply_reduce_fusion.7
  354.8 0.8 fusion.56
  355.7 1.1 fusion.57
  356.9 28.8 %all_to_all.64 = bf16[8,256,256]{2,1,0:T(8,128)(2,1)S(1)} all-to-all(bf16[8,256,256]{2,1,0:T(8,128)(2,1)S(1)} %pad_maximum_fusion.1), channel_id=1, replica_groups=mesh['sp'=8,'dp'=4] {'sp'}, dimensions={0} | all-to-all | bytes 2097152 | tf_op jit(solution)/shard_map/all_to_all | solution.py:107
  385.6 0.5 copy.27
  386.1 4.4 %all-gather.19.cloned.1.call-done = bf16[2048,2048]{0,1:T(8,128)(2,1)} async-done(((bf16[512,2048]{0,1:T(8,128)(2,1)}), bf16[2048,2048]{0,1:T(8,128)(2,1)}) %all-gather.19.cloned.1.call-update) | async-done | bytes 8388624 | tf_op jit(solution)/shard_map/all_gather | solution.py:64
  390.5 6.8 %fusion.20 = bf16[1,256,2048]{2,1,0:T(8,128)(2,1)} fusion(bf16[256,2048]{0,1:T(8,128)(2,1)S(1)} %bitcast.129, bf16[2048,2048]{0,1:T(8,128)(2,1)} %all-gather.19.cloned.1.call-done), kind=kOutput, calls=%fused_computation.29 | convolution fusion | flops 2148007936 | bytes 10485760 | tf_op jit(solution)/shard_map/dot_general | solution.py:62
  (53 shorter events, 1.4 us)
Async XLA Ops:
  6.5 171.5 %copy-start = (bf16[1,256,2048]{2,1,0:T(8,128)(2,1)S(1)}, bf16[1,256,2048]{2,1,0:T(8,128)(2,1)}, u32[]{:S(2)}) copy-start(bf16[1,256,2048]{2,1,0:T(8,128)(2,1)} %param.13) | copy-start | bytes 3145732
  6.5 46.0 %all-gather.23.cloned.1.call-start = ((), (), s32[]{:S(2)}) async-start(), calls=%async_computation.9 | async-start | bytes 1179648 | tf_op jit(solution)/shard_map/all_gather | solution.py:61
  7.3 95.2 %all-gather.21.cloned.1.call-start = ((), (), s32[]{:S(2)}) async-start(), calls=%async_computation.8 | async-start | bytes 2359296 | tf_op jit(solution)/shard_map/all_gather | solution.py:61
  8.0 135.4 %all-gather.25.cloned.1.call-start = ((), (), s32[]{:S(2)}) async-start(), calls=%async_computation.10 | async-start | bytes 1179648 | tf_op jit(solution)/shard_map/all_gather | solution.py:61
  8.7 169.3 %all-gather.15.cloned.1.call-start = ((), (), s32[]{:S(2)}) async-start(), calls=%async_computation.5 | async-start | bytes 5242880 | tf_op jit(solution)/shard_map/all_gather | solution.py:64
  54.8 183.0 %all-gather.13.cloned.1.call-start = ((), (), s32[]{:S(2)}) async-start(), calls=%async_computation.4 | async-start | bytes 10485760 | tf_op jit(solution)/shard_map/all_gather | solution.py:64
  102.4 44.1 %copy-start.5 = (f32[2,128]{1,0:T(2,128)S(1)}, f32[2,128]{1,0:T(2,128)}, u32[]{:S(2)}) copy-start(f32[2,128]{1,0:T(2,128)} %param.18) | copy-start | bytes 3076
  106.4 167.2 %all-gather.17.cloned.1.call-start = ((), (), s32[]{:S(2)}) async-start(), calls=%async_computation.6 | async-start | bytes 5242880 | tf_op jit(solution)/shard_map/all_gather | solution.py:64
  145.7 183.9 %all-gather.27.cloned.1.call-start = ((), (), s32[]{:S(2)}) async-start(), calls=%async_computation.11 | async-start | bytes 2359296 | tf_op jit(solution)/shard_map/all_gather | solution.py:61
  184.5 72.4 %all-to-all-start.1 = ((bf16[256,8,128]{2,0,1:T(8,128)(2,1)}), bf16[256,8,128]{2,0,1:T(8,128)(2,1)S(1)}, u32[]{:S(2)}, u32[]{:S(2)}) async-start(bf16[256,8,128]{2,0,1:T(8,128)(2,1)} %bitcast.22), calls=%async_computation.1 | async-start | bytes 1048576 | tf_op jit(solution)/shard_map/all_to_all | solution.py:94
  256.8 35.0 %all-to-all-start = ((bf16[256,8,256]{0,2,1:T(8,128)(2,1)}), bf16[256,8,256]{0,2,1:T(8,128)(2,1)S(1)}, u32[]{:S(2)}, u32[]{:S(2)}) async-start(bf16[256,8,256]{0,2,1:T(8,128)(2,1)} %convert_element_type.44), calls=%async_computation | async-start | bytes 2097152 | tf_op jit(solution)/shard_map/all_to_all | solution.py:87
  291.8 42.4 %all-to-all-start.2 = ((bf16[256,8,128]{2,0,1:T(8,128)(2,1)}), bf16[256,8,128]{2,0,1:T(8,128)(2,1)S(1)}, u32[]{:S(2)}, u32[]{:S(2)}) async-start(bf16[256,8,128]{2,0,1:T(8,128)(2,1)} %bitcast.28), calls=%async_computation.2 | async-start | bytes 1048576 | tf_op jit(solution)/shard_map/all_to_all | solution.py:95
  295.3 95.2 %all-gather.19.cloned.1.call-start = ((), (), s32[]{:S(2)}) async-start(), calls=%async_computation.7 | async-start | bytes 10485760 | tf_op jit(solution)/shard_map/all_gather | solution.py:64
  334.2 0.8 copy-start.2
  335.1 1.6 copy-start.3
  337.8 1.6 copy-start.3
  340.5 1.6 copy-start.3
  343.2 1.6 copy-start.3
  345.9 1.6 copy-start.4
  348.6 1.6 copy-start.4
  351.3 1.6 copy-start.4
  354.0 1.6 copy-start.4
  390.5 6.8 %copy-start.1 = (bf16[1,256,2048]{2,1,0:T(8,128)(2,1)S(1)}, bf16[1,256,2048]{2,1,0:T(8,128)(2,1)}, u32[]{:S(2)}) copy-start(bf16[1,256,2048]{2,1,0:T(8,128)(2,1)} %param.13) | copy-start | bytes 3145732
Sparse Core Ops, SparseCore 0:
  9.5 42.9 all-gather.22
  54.6 47.7 all-gather.20
  104.6 38.7 all-gather.24
  144.8 33.1 all-gather.14
  179.4 58.2 all-gather.12
  239.2 34.4 all-gather.16
  275.8 53.7 all-gather.26
  333.7 56.7 all-gather.18
